TPU v7x, 32 devices: a whole 2x2x4 slice. The times are simulated.
32 devices in a mesh: sp: 8 (over z, core), tp: 4 (over y, x).
Axes of the slice: x: 2, y: 2, z: 4, core: 2. Of those that a mesh axis runs over, the one named last changes fastest.
Arguments:
- queries: bfloat16 [4096, 1024], P('sp', 'tp'), may hold values from -20 to 20
- key_vectors: bfloat16 [4096, 1024], P('sp', 'tp'), may hold values from -20 to 20
- value_vectors: bfloat16 [4096, 1024], P('sp', 'tp'), may hold values from -6 to 6
- log_gate_sums: float32 [4096, 16], P('sp', 'tp'), may hold values from -588 to 0, as said below
- residual: bfloat16 [4096, 2048], P('sp', 'tp'), may hold values from -24 to 24
- out_weight: bfloat16 [1024, 2048], P(None, 'tp'), may hold values from -0.75 to 0.75
- norm_gain: bfloat16 [2048], replicated, may hold values from 0.099609375 to 1.8984375
- routes: int32 [4096, 2], P('sp'), may hold values from 0 to 31, all different within a row; in each aligned block of 512 rows (0 to 511, 512 to 1023, ...) at most 40 rows name the same one
- route_weight: float32 [4096, 2], P('sp'), may hold values from 0.5 to 1.5
- expert_gate: bfloat16 [32, 2048, 512], P('sp', None, 'tp'), may hold values from -0.125 to 0.125
- expert_up: bfloat16 [32, 2048, 512], P('sp', None, 'tp'), may hold values from -0.125 to 0.125
- expert_down: bfloat16 [32, 512, 2048], P('sp', None, 'tp'), may hold values from -0.25 to 0.25
- shared_gate: bfloat16 [2048, 512], P(None, 'tp'), may hold values from -0.125 to 0.125
- shared_up: bfloat16 [2048, 512], P(None, 'tp'), may hold values from -0.125 to 0.125
- shared_down: bfloat16 [512, 2048], P(None, 'tp'), may hold values from -0.25 to 0.25
Outputs:
- layer_out: bfloat16 [4096, 2048], P('sp', 'tp')
Inputs may be any that keep to these rules, and one draw needn't show every extreme that they name: `log_gate_sums`: for each head the values do not rise along the positions. `routes`: each row names 2 different experts; among the rows of one index of sp no expert is named by more than 40 rows, a bound that some block reaches.
All inputs are finite; a program needn't handle non-finite values.
Results may differ from a plain program's by a relative error of at most 0.014.
Values may be sent and summed in bfloat16 or wider, within the bound.
A program may use at most 64 MiB of HBM per device.

v0:
```python
import math

import jax
import jax.numpy as jnp
from jax import lax
from jax.sharding import PartitionSpec as P

HDIM = 64


EPSILON = 1e-06


def silu_gate(gate_part, up_part):
    return jax.nn.silu(gate_part) * up_part


def slot_targets(routes, experts_all, capacity):
    flat_routes = routes.reshape(-1)
    onehot = (flat_routes[:, None] == jnp.arange(experts_all, dtype=jnp.int32)[None, :]).astype(
        jnp.int32
    )
    before = jnp.cumsum(onehot, axis=0) - onehot
    return flat_routes * capacity + jnp.sum(before * onehot, axis=1)


def keep_state(fold_state):
    return fold_state


def shards(
    queries,
    key_vectors,
    value_vectors,
    log_gate_sums,
    residual,
    out_weight,
    norm_gain,
    routes,
    route_weight,
    expert_gate,
    expert_up,
    expert_down,
    shared_gate,
    shared_up,
    shared_down,
):
    tok_dev = queries.shape[0]
    head_dim = HDIM
    local_heads = log_gate_sums.shape[1]
    local_width = residual.shape[1]
    model_width = norm_gain.shape[0]
    score_scale = head_dim ** (-0.5)
    seq_first = lax.axis_index("sp") * tok_dev
    query_heads = queries.reshape(tok_dev, local_heads, head_dim)
    query_pos = seq_first + jnp.arange(tok_dev, dtype=jnp.int32)
    own_gates = log_gate_sums.T
    all_gates = lax.all_gather(log_gate_sums, "sp", axis=0, tiled=True)
    initial = (
        jnp.full((local_heads, tok_dev), -1e30, jnp.float32),
        jnp.zeros((local_heads, tok_dev), jnp.float32),
        jnp.zeros((local_heads, tok_dev, head_dim), jnp.float32),
    )
    key_heads = key_vectors.reshape(tok_dev, local_heads, head_dim)
    value_heads = value_vectors.reshape(tok_dev, local_heads, head_dim)
    key_part = lax.all_gather(key_heads, "sp", axis=0, tiled=True)
    value_part = lax.all_gather(value_heads, "sp", axis=0, tiled=True)
    part_rows = key_part.shape[0]
    block_size = math.gcd(part_rows, 512)
    key_blocks = key_part.reshape(part_rows // block_size, block_size, local_heads, head_dim)
    value_blocks = value_part.reshape(part_rows // block_size, block_size, local_heads, head_dim)

    def one_block(fold_state, inputs):
        key_block, value_block, block_number = inputs
        block_first = block_number * block_size

        def compute(old_state):
            running_max, weight_total, summed = old_state
            gate_block = lax.dynamic_slice_in_dim(all_gates, block_first, block_size, 0).T
            scores = (
                jnp.einsum(
                    "qhd,khd->hqk", query_heads, key_block, preferred_element_type=jnp.float32
                )
                * score_scale
            )
            scores = scores + own_gates[:, :, None] - gate_block[:, None, :]
            key_pos = block_first + jnp.arange(block_size, dtype=jnp.int32)
            allowed = (key_pos[None, :] <= query_pos[:, None])[None]
            newmax = jnp.maximum(running_max, jnp.max(jnp.where(allowed, scores, -jnp.inf), axis=2))
            factor = jnp.exp(running_max - newmax)
            weight = jnp.where(allowed, jnp.exp(scores - newmax[:, :, None]), 0.0)
            weight_total = weight_total * factor + jnp.sum(weight, axis=2)
            summed = summed * factor[:, :, None] + jnp.einsum(
                "hqk,khd->hqd",
                weight.astype(jnp.bfloat16),
                value_block,
                preferred_element_type=jnp.float32,
            )
            return (newmax, weight_total, summed)

        useful = block_first <= seq_first + tok_dev - 1
        return (lax.cond(useful, compute, keep_state, fold_state), None)

    numbers = jnp.arange(part_rows // block_size, dtype=jnp.int32)
    result_state, _ = lax.scan(one_block, initial, (key_blocks, value_blocks, numbers))
    running_max, weight_total, summed = result_state
    attended = (summed / weight_total[:, :, None]).astype(jnp.bfloat16)
    attended = attended.transpose(1, 0, 2).reshape(tok_dev, local_heads * head_dim)
    weight_rows = out_weight
    projected = jnp.dot(
        lax.all_gather(attended, "tp", axis=1, tiled=True),
        weight_rows,
        preferred_element_type=jnp.float32,
    )
    mid = (residual.astype(jnp.float32) + projected).astype(jnp.bfloat16)
    mid_wide = mid.astype(jnp.float32)
    feature_first = lax.axis_index("tp") * local_width
    squares = lax.psum(jnp.sum(mid_wide * mid_wide, axis=1), "tp")
    inverse = lax.rsqrt(squares / model_width + EPSILON)
    own_gain = lax.dynamic_slice_in_dim(norm_gain, feature_first, local_width, 0).astype(
        jnp.float32
    )
    normed_own = (mid_wide * inverse[:, None] * own_gain[None, :]).astype(jnp.bfloat16)
    normed = lax.all_gather(normed_own, "tp", axis=1, tiled=True)
    shared_mid = silu_gate(
        jnp.dot(normed, shared_gate, preferred_element_type=jnp.float32),
        jnp.dot(normed, shared_up, preferred_element_type=jnp.float32),
    ).astype(jnp.bfloat16)
    weight_rows = shared_down
    shared_out = jnp.dot(
        lax.all_gather(shared_mid, "tp", axis=1, tiled=True),
        weight_rows,
        preferred_element_type=jnp.float32,
    )
    exp_dev = expert_gate.shape[0]
    sp_count = lax.axis_size("sp")
    experts_all = exp_dev * sp_count
    top_count = routes.shape[1]
    capacity = 5 * tok_dev * top_count // (4 * experts_all)
    targets = slot_targets(routes, experts_all, capacity)
    owners = (
        jnp.full((experts_all * capacity,), tok_dev, jnp.int32)
        .at[targets]
        .set(jnp.arange(tok_dev * top_count, dtype=jnp.int32) // top_count)
    )
    padded = jnp.concatenate(
        [normed_own, jnp.zeros((1, normed_own.shape[1]), jnp.bfloat16)], axis=0
    )
    outgoing = padded[owners].reshape(sp_count, exp_dev, capacity, normed_own.shape[1])
    rows_all = lax.all_gather(
        lax.all_to_all(outgoing, "sp", split_axis=0, concat_axis=0, tiled=True),
        "tp",
        axis=3,
        tiled=True,
    )
    gate_part = jnp.einsum(
        "secd,edf->secf", rows_all, expert_gate, preferred_element_type=jnp.float32
    )
    up_part = jnp.einsum("secd,edf->secf", rows_all, expert_up, preferred_element_type=jnp.float32)
    hidden = silu_gate(gate_part, up_part).astype(jnp.bfloat16)
    hidden_all = lax.all_gather(hidden, "tp", axis=3, tiled=True)
    produced = jnp.einsum(
        "secf,efd->secd", hidden_all, expert_down, preferred_element_type=jnp.float32
    ).astype(jnp.bfloat16)
    returned = lax.all_to_all(produced, "sp", split_axis=0, concat_axis=0, tiled=True)
    returned_flat = returned.reshape(experts_all * capacity, local_width)
    picked = returned_flat[targets].astype(jnp.float32).reshape(tok_dev, top_count, local_width)
    routed = jnp.sum(picked * route_weight[:, :, None], axis=1)
    return (mid_wide + shared_out + routed).astype(jnp.bfloat16)


def solution(mesh):
    placed = (
        P("sp", "tp"),
        P("sp", "tp"),
        P("sp", "tp"),
        P("sp", "tp"),
        P("sp", "tp"),
        P(None, "tp"),
        P(),
        P("sp", None),
        P("sp", None),
        P("sp", None, "tp"),
        P("sp", None, "tp"),
        P("sp", None, "tp"),
        P(None, "tp"),
        P(None, "tp"),
        P(None, "tp"),
    )
    return jax.shard_map(
        shards, mesh=mesh, in_specs=placed, out_specs=P("sp", "tp"), check_vma=False
    )
```

profile of v0, /device:TPU:9, one launch (start us, length us, event | category | flops | bytes accessed | tf_op | source)
XLA Modules:
  0.0 380.0 jit_solution(4985606902853403032)
XLA Ops:
  11.8 15.0 %all_gather.25 = f32[4096,4]{0,1:T(4,128)S(1)} all-gather(f32[512,4]{0,1:T(4,128)S(1)} %copy-done.9), channel_id=1, replica_groups=mesh['sp'=8,'tp'=4] {'sp'}, dimensions={0}, use_global_device_ids=true | all-gather | bytes 73728 | tf_op jit(solution)/shard_map/all_gather | solution.py:58
  26.8 13.2 %all-gather.9.cloned.1.call-done = bf16[4096,4,64]{0,2,1:T(8,128)(2,1)} async-done(((bf16[512,4,64]{0,2,1:T(8,128)(2,1)}), bf16[4096,4,64]{0,2,1:T(8,128)(2,1)}) %all-gather.9.cloned.1.call-update) | async-done | bytes 2097168 | tf_op jit(solution)/shard_map/all_gather | solution.py:67
  39.9 3.2 copy.57
  43.1 27.0 %all-gather.7.cloned.1.call-done = bf16[4096,4,64]{0,2,1:T(8,128)(2,1)} async-done(((bf16[512,4,64]{0,2,1:T(8,128)(2,1)}), bf16[4096,4,64]{0,2,1:T(8,128)(2,1)}) %all-gather.7.cloned.1.call-update) | async-done | bytes 2097168 | tf_op jit(solution)/shard_map/all_gather | solution.py:66
  70.1 3.2 copy.58
  73.4 35.5 %while.17 = (s32[]{:T(128)}, f32[4,512]{1,0:T(4,128)S(1)}, f32[4,512]{1,0:T(4,128)S(1)}, f32[4,512,64]{1,2,0:T(8,128)S(1)}, s32[8]{0:T(128)S(1)}, /*index=5*/s32...) while((s32[]{:T(128)}, f32[4,512]{1,0:T(4,128)S(1)}, ...), condition=%wide.region_5.6_spmd.clone, body=%wide.region_0.5_spmd.clone.sunk | while | flops 286790656 | bytes 15676785 | solution.py:105
  74.7 6.3 %conditional.3 = ((f32[4,512]{1,0:T(4,128)S(1)}, f32[4,512]{1,0:T(4,128)S(1)}, f32[4,512,64]{1,2,0:T(8,128)S(1)})) conditional(s32[]{:T(128)} %convert_element_type.105, (f32[4,512]{1,0:T(4,128)S(1)}, f32[4,512]{1,0:T(4,128)S(1)}, f32[4,512,64]{1,2,0:T(8,128)S(1)}) %tuple.50, (s32[]{:T(128)}, s32[]{:T(128)}, bf16[8,512,4,64]{1,3,2,0:T(8,128)(2,1)}, ...), branch_computations={%region_1.1_spmd, %region_2.4_spmd} | conditional | flops 286790656 | bytes 15674446 | solution.py:102
  78.6 2.3 fusion.10
  82.2 6.3 %conditional.3 = ((f32[4,512]{1,0:T(4,128)S(1)}, f32[4,512]{1,0:T(4,128)S(1)}, f32[4,512,64]{1,2,0:T(8,128)S(1)})) conditional(s32[]{:T(128)} %convert_element_type.105, (f32[4,512]{1,0:T(4,128)S(1)}, f32[4,512]{1,0:T(4,128)S(1)}, f32[4,512,64]{1,2,0:T(8,128)S(1)}) %tuple.50, (s32[]{:T(128)}, s32[]{:T(128)}, bf16[8,512,4,64]{1,3,2,0:T(8,128)(2,1)}, ...), branch_computations={%region_1.1_spmd, %region_2.4_spmd} | conditional | flops 286790656 | bytes 15674446 | solution.py:102
  86.2 2.3 fusion.10
  89.8 6.3 %conditional.3 = ((f32[4,512]{1,0:T(4,128)S(1)}, f32[4,512]{1,0:T(4,128)S(1)}, f32[4,512,64]{1,2,0:T(8,128)S(1)})) conditional(s32[]{:T(128)} %convert_element_type.105, (f32[4,512]{1,0:T(4,128)S(1)}, f32[4,512]{1,0:T(4,128)S(1)}, f32[4,512,64]{1,2,0:T(8,128)S(1)}) %tuple.50, (s32[]{:T(128)}, s32[]{:T(128)}, bf16[8,512,4,64]{1,3,2,0:T(8,128)(2,1)}, ...), branch_computations={%region_1.1_spmd, %region_2.4_spmd} | conditional | flops 286790656 | bytes 15674446 | solution.py:102
  93.8 2.3 fusion.10
  97.4 6.3 %conditional.3 = ((f32[4,512]{1,0:T(4,128)S(1)}, f32[4,512]{1,0:T(4,128)S(1)}, f32[4,512,64]{1,2,0:T(8,128)S(1)})) conditional(s32[]{:T(128)} %convert_element_type.105, (f32[4,512]{1,0:T(4,128)S(1)}, f32[4,512]{1,0:T(4,128)S(1)}, f32[4,512,64]{1,2,0:T(8,128)S(1)}) %tuple.50, (s32[]{:T(128)}, s32[]{:T(128)}, bf16[8,512,4,64]{1,3,2,0:T(8,128)(2,1)}, ...), branch_computations={%region_1.1_spmd, %region_2.4_spmd} | conditional | flops 286790656 | bytes 15674446 | solution.py:102
  101.4 2.3 fusion.10
  109.7 9.0 %reduce-window.6 = s32[32,8,128]{2,1,0:T(8,128)S(1)} reduce-window(s32[32,8,128]{2,1,0:T(8,128)S(1)} %fusion.56, s32[]{:T(128)} %constant.93.clone.1), window={size=1x1x128 pad=0_0x0_0x127_0}, to_apply=%region_8.9 | reduce-window | flops 4161536 | bytes 262148 | tf_op jit(solution)/shard_map/reduce-window
  119.6 4.3 %scatter_custom_fusion = s32[1280]{0:T(1024)S(1)} fusion(s32[1024]{0:T(1024)S(1)} %bitcast.129, s32[1024]{0:T(1024)S(1)} %add_select_fusion, s32[]{:T(128)} %constant.98.clone.1), kind=kCustom, calls=%fused_computation.75 | custom fusion | bytes 5124 | tf_op jit(solution)/shard_map/scatter | solution.py:144
  124.7 35.5 %all-gather.11.cloned.1.call-done = bf16[512,1024]{0,1:T(8,128)(2,1)} async-done(((bf16[512,256]{0,1:T(8,128)(2,1)}), bf16[512,1024]{0,1:T(8,128)(2,1)}) %all-gather.11.cloned.1.call-update) | async-done | bytes 1048592 | tf_op jit(solution)/shard_map/all_gather | solution.py:111
  160.2 2.5 fusion.50
  162.7 6.9 %psum.7 = f32[512]{0:T(512)S(1)} all-reduce(f32[512]{0:T(512)S(1)} %get-tuple-element.335), channel_id=1, replica_groups=mesh['sp'=8,'tp'=4] {'tp'}, use_global_device_ids=true, to_apply=%region_7.8 | all-reduce | flops 512 | bytes 4096 | tf_op jit(solution)/shard_map/psum | solution.py:118
  169.9 4.7 %gather_fusion = bf16[1280,512]{1,0:T(8,128)(2,1)} fusion(bf16[513,512]{1,0:T(8,128)(2,1)S(1)} %concatenate.3, s32[2048]{0:T(1024)S(1)} %pad_clamp_fusion), kind=kCustom, calls=%fused_computation | custom fusion | bytes 2626560 | tf_op jit(solution)/shard_map/gather | solution.py:149
  174.6 36.8 %all_to_all.10 = bf16[8,4,40,512]{3,2,1,0:T(8,128)(2,1)S(1)} all-to-all(bf16[8,4,40,512]{3,2,1,0:T(8,128)(2,1)} %bitcast.116), channel_id=1, replica_groups=mesh['sp'=8,'tp'=4] {'sp'}, dimensions={0} | all-to-all | bytes 2621440 | tf_op jit(solution)/shard_map/all_to_all | solution.py:151
  212.9 61.1 %all-gather.15.cloned.1.call-done = bf16[8,4,40,2048]{3,2,0,1:T(8,128)(2,1)} async-done(((bf16[8,4,40,512]{3,2,0,1:T(8,128)(2,1)}), bf16[8,4,40,2048]{3,2,0,1:T(8,128)(2,1)}) %all-gather.15.cloned.1.call-update) | async-done | bytes 5242896 | tf_op jit(solution)/shard_map/all_gather | solution.py:150
  273.9 4.8 %fusion.37 = f32[8,4,40,128]{3,2,0,1:T(8,128)S(1)} fusion(bf16[8,4,40,2048]{3,2,0,1:T(8,128)(2,1)} %all-gather.15.cloned.1.call-done, bf16[4,2048,128]{2,1,0:T(8,128)(2,1)} %param.28), kind=kOutput, calls=%fused_computation.48 | convolution fusion | flops 671088640 | bytes 7995392 | tf_op jit(solution)/shard_map/secd,edf->secf/dot_general | solution.py:156
  279.3 2.3 fusion.46
  282.1 28.1 %all-gather.17.cloned.1.call-done = bf16[8,4,40,512]{3,2,0,1:T(8,128)(2,1)} async-done(((bf16[8,4,40,128]{3,2,0,1:T(8,128)(2,1)}), bf16[8,4,40,512]{3,2,0,1:T(8,128)(2,1)}) %all-gather.17.cloned.1.call-update) | async-done | bytes 1310736 | tf_op jit(solution)/shard_map/all_gather | solution.py:161
  313.6 5.6 %all-to-all-start.1 = ((bf16[8,4,40,512]{3,2,1,0:T(8,128)(2,1)}), bf16[8,4,40,512]{3,2,1,0:T(8,128)(2,1)S(1)}, u32[]{:S(2)}, u32[]{:S(2)}) async-start(bf16[8,4,40,512]{3,2,1,0:T(8,128)(2,1)} %copy.45), calls=%async_computation.1 | async-start | bytes 2621440 | tf_op jit(solution)/shard_map/all_to_all | solution.py:165
  320.1 26.9 %all-gather.13.cloned.1.call-done = bf16[512,2048]{1,0:T(8,128)(2,1)} async-done(((bf16[512,512]{1,0:T(8,128)(2,1)}), bf16[512,2048]{1,0:T(8,128)(2,1)}) %all-gather.13.cloned.1.call-update) | async-done | bytes 2097168 | tf_op jit(solution)/shard_map/all_gather | solution.py:124
  347.0 2.5 fusion.62
  350.3 8.6 %all_gather.29 = bf16[512,512]{1,0:T(8,128)(2,1)} all-gather(bf16[512,128]{1,0:T(8,128)(2,1)S(1)} %fusion.49), channel_id=1, replica_groups=mesh['sp'=8,'tp'=4] {'tp'}, dimensions={1}, use_global_device_ids=true | all-gather | bytes 655360 | tf_op jit(solution)/shard_map/all_gather | solution.py:131
  358.9 5.1 %gather_fusion.1 = bf16[1024,512]{1,0:T(8,128)(2,1)} fusion(bf16[1280,512]{1,0:T(8,128)(2,1)S(1)} %bitcast.115, s32[1024]{0:T(1024)S(1)} %broadcast_clamp_fusion), kind=kCustom, calls=%fused_computation.1 | custom fusion | bytes 2101248 | tf_op jit(solution)/shard_map/gather | solution.py:167
  363.9 3.4 reshape.124
  367.4 4.5 %multiply_reduce_fusion = f32[512,512]{1,0:T(8,128)S(1)} fusion(f32[512,2,512]{2,1,0:T(2,128)} %reshape.124, f32[512,2]{1,0:T(8,128)S(1)} %copy-done.7), kind=kLoop, calls=%fused_computation.38 | loop fusion | flops 786432 | bytes 3149824 | tf_op jit(solution)/shard_map/reduce_sum | solution.py:168
  (132 shorter events, 37.0 us)
Async XLA Ops:
  6.5 303.7 %copy-start = (bf16[4,512,512]{2,1,0:T(8,128)(2,1)S(1)}, bf16[4,512,512]{2,1,0:T(8,128)(2,1)}, u32[]{:S(2)}) copy-start(bf16[4,512,512]{2,1,0:T(8,128)(2,1)} %param.30) | copy-start | bytes 6291460
  6.5 5.1 %copy-start.10 = (bf16[512,256]{1,0:T(8,128)(2,1)S(1)}, bf16[512,256]{1,0:T(8,128)(2,1)}, u32[]{:S(2)}) copy-start(bf16[512,256]{1,0:T(8,128)(2,1)} %param.19) | copy-start | bytes 786436
  6.5 5.2 %copy-start.9 = (f32[512,4]{0,1:T(4,128)S(1)}, f32[512,4]{0,1:T(4,128)}, u32[]{:S(2)}) copy-start(f32[512,4]{0,1:T(4,128)} %param.22) | copy-start | bytes 24580
  6.5 33.4 %all-gather.9.cloned.1.call-start = ((), (), s32[]{:S(2)}) async-start(), calls=%async_computation.3 | async-start | bytes 2359296 | tf_op jit(solution)/shard_map/all_gather | solution.py:67
  8.5 61.6 %all-gather.7.cloned.1.call-start = ((), (), s32[]{:S(2)}) async-start(), calls=%async_computation.2 | async-start | bytes 2359296 | tf_op jit(solution)/shard_map/all_gather | solution.py:66
  10.4 149.8 %all-gather.11.cloned.1.call-start = ((), (), s32[]{:S(2)}) async-start(), calls=%async_computation.4 | async-start | bytes 1310720 | tf_op jit(solution)/shard_map/all_gather | solution.py:111
  73.4 45.7 %copy-start.11 = (s32[512,2]{0,1:T(2,128)S(1)}, s32[512,2]{0,1:T(2,128)}, u32[]{:S(2)}) copy-start(s32[512,2]{0,1:T(2,128)} %param.26) | copy-start | bytes 12292
  109.6 164.3 %all-gather.15.cloned.1.call-start = ((), (), s32[]{:S(2)}) async-start(), calls=%async_computation.6 | async-start | bytes 6553600 | tf_op jit(solution)/shard_map/all_gather | solution.py:150
  162.7 7.1 %copy-start.5 = (bf16[512,512]{1,0:T(8,128)(2,1)}, bf16[512,512]{1,0:T(8,128)(2,1)S(1)}, u32[]{:S(2)}) copy-start(bf16[512,512]{1,0:T(8,128)(2,1)S(1)} %get-tuple-element.336) | copy-start | bytes 1572868
  169.8 4.8 %copy-start.2 = (bf16[512,512]{1,0:T(8,128)(2,1)}, bf16[512,512]{1,0:T(8,128)(2,1)S(1)}, u32[]{:S(2)}) copy-start(bf16[512,512]{1,0:T(8,128)(2,1)S(1)} %fusion.52) | copy-start | bytes 1572868
  212.7 97.6 %all-gather.17.cloned.1.call-start = ((), (), s32[]{:S(2)}) async-start(), calls=%async_computation.7 | async-start | bytes 1638400 | tf_op jit(solution)/shard_map/all_gather | solution.py:161
  273.9 4.8 %copy-start.1 = (bf16[8,4,40,2048]{3,2,0,1:T(8,128)(2,1)S(1)}, bf16[8,4,40,2048]{3,2,0,1:T(8,128)(2,1)}, u32[]{:S(2)}) copy-start(bf16[8,4,40,2048]{3,2,0,1:T(8,128)(2,1)} %all-gather.15.cloned.1.call-done) | copy-start | bytes 15728644
  273.9 5.3 %copy-start.13 = (bf16[4,2048,128]{2,1,0:T(8,128)(2,1)S(1)}, bf16[4,2048,128]{2,1,0:T(8,128)(2,1)}, u32[]{:S(2)}) copy-start(bf16[4,2048,128]{2,1,0:T(8,128)(2,1)} %param.29) | copy-start | bytes 6291460
  281.5 65.4 %all-gather.13.cloned.1.call-start = ((), (), s32[]{:S(2)}) async-start(), calls=%async_computation.5 | async-start | bytes 2621440 | tf_op jit(solution)/shard_map/all_gather | solution.py:124
  312.4 6.8 %copy-start.12 = (f32[512,2]{0,1:T(2,128)S(1)}, f32[512,2]{0,1:T(2,128)}, u32[]{:S(2)}) copy-start(f32[512,2]{0,1:T(2,128)} %param.27) | copy-start | bytes 12292
  313.6 45.3 %all-to-all-start.1 = ((bf16[8,4,40,512]{3,2,1,0:T(8,128)(2,1)}), bf16[8,4,40,512]{3,2,1,0:T(8,128)(2,1)S(1)}, u32[]{:S(2)}, u32[]{:S(2)}) async-start(bf16[8,4,40,512]{3,2,1,0:T(8,128)(2,1)} %copy.45), calls=%async_computation.1 | async-start | bytes 2621440 | tf_op jit(solution)/shard_map/all_to_all | solution.py:165
  347.0 2.5 copy-start.3
  347.0 2.6 copy-start.14
  363.9 3.4 copy-start.7
  367.4 4.5 %copy-start.4 = (bf16[512,512]{1,0:T(8,128)(2,1)S(1)}, bf16[512,512]{1,0:T(8,128)(2,1)}, u32[]{:S(2)}) copy-start(bf16[512,512]{1,0:T(8,128)(2,1)} %all_gather.29) | copy-start | bytes 1572868
  367.4 4.5 %copy-start.6 = (bf16[512,512]{1,0:T(8,128)(2,1)S(1)}, bf16[512,512]{1,0:T(8,128)(2,1)}, u32[]{:S(2)}) copy-start(bf16[512,512]{1,0:T(8,128)(2,1)} %copy-done.5) | copy-start | bytes 1572868
  367.4 4.6 %copy-start.8 = (bf16[512,512]{1,0:T(8,128)(2,1)S(1)}, bf16[512,512]{1,0:T(8,128)(2,1)}, u32[]{:S(2)}) copy-start(bf16[512,512]{1,0:T(8,128)(2,1)} %param.33) | copy-start | bytes 1572868
Sparse Core Ops, SparseCore 0:
  8.9 30.9 all-gather.8
  41.5 28.5 all-gather.6
  109.7 50.3 all-gather.10
  212.8 61.1 all-gather.14
  281.7 28.5 all-gather.16
  311.9 35.0 all-gather.12
where the time goes:
time: 385 us; the launch traced here: 380 us
  waiting for transfers between devices  192 us (50%)
  blocking collectives  67.3 us (17%)
  local copies, waits for them, and re-layouts  38.5 us (10%)
  matrix products  34.4 us (9%)
  other arithmetic  21.9 us (6%)
  between operations  13.8 us (4%)
  starting transfers between devices  5.98 us (2%)
  loops' own time  5.81 us (2%)
    all_gather x1, waiting for transfers between devices, shards(): lax.all_gather(lax.all_to_all(outgoing, 'sp', split_axis=0, concat_axis=0...  61.1 us
    all_to_all x1, blocking collectives, shards(): lax.all_to_all(outgoing, 'sp', split_axis=0, concat_axis=0, tiled=True)  36.8 us
    all_gather x1, waiting for transfers between devices, shards(): lax.all_gather(attended, 'tp', axis=1, tiled=True)  35.5 us
    all_gather x1, waiting for transfers between devices, shards(): hidden_all = lax.all_gather(hidden, 'tp', axis=3, tiled=True)  28.1 us
    all_gather x1, waiting for transfers between devices, shards(): key_part = lax.all_gather(key_heads, 'sp', axis=0, tiled=True)  27 us
    all_gather x1, waiting for transfers between devices, shards(): normed = lax.all_gather(normed_own, 'tp', axis=1, tiled=True)  26.9 us
    all_gather x1, blocking collectives, shards(): all_gates = lax.all_gather(log_gate_sums, 'sp', axis=0, tiled=True)  15 us
    all_gather x1, waiting for transfers between devices, shards(): value_part = lax.all_gather(value_heads, 'sp', axis=0, tiled=True)  13.2 us
  transfers between devices with their start and end apart: 7, of which 6 were waited for; matrix products, arithmetic and copies ran while one was open for 8% of the time, Pallas kernels for 0%

commit v1 on v0

--- a/solution.py
+++ b/solution.py
@@ -1,8 +1,11 @@
+import functools
 import math
 
 import jax
 import jax.numpy as jnp
 from jax import lax
+from jax.experimental import pallas as pl
+from jax.experimental.pallas import tpu as pltpu
 from jax.sharding import PartitionSpec as P
 
 HDIM = 64
@@ -169,6 +172,619 @@
     return (mid_wide + shared_out + routed).astype(jnp.bfloat16)
 
 
+def peer(sp=None, tp=None):
+    named = {}
+    if sp is not None:
+        named["sp"] = sp
+    if tp is not None:
+        named["tp"] = tp
+    return named
+
+
+def send(src, dst, send_sem, recv_sem, to):
+    return pltpu.make_async_remote_copy(
+        src_ref=src,
+        dst_ref=dst,
+        send_sem=send_sem,
+        recv_sem=recv_sem,
+        device_id=to,
+        device_id_type=pl.DeviceIdType.MESH,
+    )
+
+
+def greet(to):
+    pl.semaphore_signal(
+        pltpu.get_barrier_semaphore(), inc=1, device_id=to, device_id_type=pl.DeviceIdType.MESH
+    )
+
+
+def kv_kernel(
+    n_sp,
+    k_ref,
+    v_ref,
+    g_ref,
+    gate_ref,
+    up_ref,
+    k_all,
+    v_all,
+    g_all,
+    gate_all,
+    up_all,
+    up_send,
+    up_recv,
+    side_send,
+    side_recv,
+    w_send,
+    w_recv,
+    own_sem,
+):
+    me = lax.axis_index("sp")
+    tp = lax.axis_index("tp")
+    z, core = me // 2, me % 2
+    depth = n_sp // 2
+    partner = z * 2 + (1 - core)
+    has_above = z + 1 < depth
+    greet(peer(sp=partner))
+    for d in range(1, 4):
+        greet(peer(tp=(tp + d) % 4))
+
+    @pl.when(has_above)
+    def _():
+        greet(peer(sp=(me + 2) % n_sp))
+
+    @pl.when(z > 0)
+    def _():
+        greet(peer(sp=(me - 2 + n_sp) % n_sp))
+
+    count = 4 + jnp.where(has_above, 1, 0) + jnp.where(z > 0, 1, 0)
+    pl.semaphore_wait(pltpu.get_barrier_semaphore(), count)
+    above = peer(sp=(me + 2) % n_sp)
+    blocks = (k_ref, v_ref, g_ref)
+    wholes = (k_all, v_all, g_all)
+
+    def upward(s, i):
+        slot = ((z - s + depth) % depth) * 2 + core
+        src = blocks[i] if s == 0 else wholes[i].at[slot]
+        return send(src, wholes[i].at[slot], up_send.at[s, i], up_recv.at[s, i], above)
+
+    def arriving(s, i):
+        slot = ((z - 1 - s + 2 * depth) % depth) * 2 + core
+        return send(blocks[i], wholes[i].at[slot], up_send.at[s, i], up_recv.at[s, i], above)
+
+    def sideways(s, i):
+        slot = ((z - s + depth) % depth) * 2 + core
+        src = blocks[i] if s == 0 else wholes[i].at[slot]
+        return send(src, wholes[i].at[slot], side_send.at[s, i], side_recv.at[s, i], peer(sp=partner))
+
+    def from_side(s, i):
+        slot = ((z - s + depth) % depth) * 2 + (1 - core)
+        return send(
+            blocks[i], wholes[i].at[slot], side_send.at[s, i], side_recv.at[s, i], peer(sp=partner)
+        )
+
+    weights = ((gate_ref, gate_all), (up_ref, up_all))
+
+    def weight_out(d, i):
+        to = (tp + d) % 4
+        return send(
+            weights[i][0].at[to],
+            weights[i][1].at[tp],
+            w_send.at[d - 1, i],
+            w_recv.at[d - 1, i],
+            peer(tp=to),
+        )
+
+    def weight_in(d, i):
+        source = (tp - d + 4) % 4
+        return send(
+            weights[i][0].at[source],
+            weights[i][1].at[source],
+            w_send.at[d - 1, i],
+            w_recv.at[d - 1, i],
+            peer(tp=source),
+        )
+
+    three = range(3)
+
+    @pl.when(has_above)
+    def _():
+        for i in three:
+            upward(0, i).start()
+
+    for i in three:
+        sideways(0, i).start()
+    for d in (2, 1, 3):
+        for i in range(2):
+            weight_out(d, i).start()
+    own = [pltpu.make_async_copy(blocks[i], wholes[i].at[me], own_sem.at[i]) for i in three]
+    for copy in own:
+        copy.start()
+    for s in range(1, depth):
+
+        @pl.when(z >= s)
+        def _():
+            for i in three:
+                arriving(s - 1, i).wait_recv()
+                if s < depth - 1:
+
+                    @pl.when(has_above)
+                    def _():
+                        upward(s, i).start()
+
+                sideways(s, i).start()
+
+    for s in range(depth):
+
+        @pl.when(z >= s)
+        def _():
+            for i in three:
+                from_side(s, i).wait_recv()
+                sideways(s, i).wait_send()
+            if s < depth - 1:
+
+                @pl.when(has_above)
+                def _():
+                    for i in three:
+                        upward(s, i).wait_send()
+
+    for copy in own:
+        copy.wait()
+    for d in range(1, 4):
+        for i in range(2):
+            weight_in(d, i).wait_recv()
+            weight_out(d, i).wait_send()
+
+
+def gather_kernel(block, whole, send_sem, recv_sem, own_sem):
+    tp = lax.axis_index("tp")
+    rows, width = block.shape
+    half = rows // 2
+    x_near = tp // 2 * 2 + (1 - tp % 2)
+    y_near = (tp + 2) % 4
+    nears = (x_near, y_near)
+    for near in nears:
+        greet(peer(tp=near))
+    pl.semaphore_wait(pltpu.get_barrier_semaphore(), 2)
+
+    def place(owner, part):
+        return whole.at[pl.ds(part * half, half), pl.ds(pl.multiple_of(owner * width, width), width)]
+
+    def outward(axis, part):
+        return send(
+            block.at[pl.ds(part * half, half)],
+            place(tp, part),
+            send_sem.at[axis, part],
+            recv_sem.at[axis, part],
+            peer(tp=nears[axis]),
+        )
+
+    def inward(axis, part):
+        return send(
+            block.at[pl.ds(part * half, half)],
+            place(nears[axis], part),
+            send_sem.at[axis, part],
+            recv_sem.at[axis, part],
+            peer(tp=nears[axis]),
+        )
+
+    far = (x_near + 2) % 4
+
+    def relay(axis):
+        return send(
+            place(nears[1 - axis], axis),
+            place(nears[1 - axis], axis),
+            send_sem.at[axis, 2],
+            recv_sem.at[axis, 2],
+            peer(tp=nears[axis]),
+        )
+
+    def relayed(axis):
+        return send(
+            place(far, axis),
+            place(far, axis),
+            send_sem.at[axis, 2],
+            recv_sem.at[axis, 2],
+            peer(tp=nears[axis]),
+        )
+
+    for order in range(2):
+        for axis in range(2):
+            outward(axis, (1 - axis + order) % 2).start()
+    own = pltpu.make_async_copy(
+        block, whole.at[:, pl.ds(pl.multiple_of(tp * width, width), width)], own_sem
+    )
+    own.start()
+    for axis in range(2):
+        inward(1 - axis, axis).wait_recv()
+        relay(axis).start()
+    for axis in range(2):
+        inward(axis, 1 - (1 - axis)).wait_recv()
+        relayed(axis).wait_recv()
+        relay(axis).wait_send()
+        for part in range(2):
+            outward(axis, part).wait_send()
+    own.wait()
+
+
+def any_space(count):
+    return [pl.BlockSpec(memory_space=pl.ANY)] * count
+
+
+def vmem_space(count):
+    return [pl.BlockSpec(memory_space=pltpu.VMEM)] * count
+
+
+def gather_features(block, number):
+    rows, width = block.shape
+    return pl.pallas_call(
+        gather_kernel,
+        name=f"gather_{number}",
+        out_shape=jax.ShapeDtypeStruct((rows, 4 * width), block.dtype),
+        in_specs=vmem_space(1),
+        out_specs=pl.BlockSpec(memory_space=pl.ANY),
+        scratch_shapes=[
+            pltpu.SemaphoreType.DMA((2, 3)),
+            pltpu.SemaphoreType.DMA((2, 3)),
+            pltpu.SemaphoreType.DMA,
+        ],
+        compiler_params=pltpu.CompilerParams(collective_id=number, has_side_effects=True),
+    )(block)
+
+
+def dispatch_kernel(
+    n_sp, rows, mid, down, rows_all, mid_all, down_all, z_send, z_recv, t_send, t_recv, own_sem
+):
+    me = lax.axis_index("sp")
+    tp = lax.axis_index("tp")
+    width = mid.shape[1]
+    for d in range(1, n_sp):
+        greet(peer(sp=(me + d) % n_sp))
+    for d in range(1, 4):
+        greet(peer(tp=(tp + d) % 4))
+    pl.semaphore_wait(pltpu.get_barrier_semaphore(), n_sp - 1 + 3)
+
+    def columns(owner):
+        return mid_all.at[:, pl.ds(pl.multiple_of(owner * width, width), width)]
+
+    def row_copy(d):
+        to = (me + d) % n_sp
+        return send(rows.at[to], rows_all.at[me], z_send.at[d], z_recv.at[d], peer(sp=to))
+
+    def row_arrival(d):
+        source = (me - d + n_sp) % n_sp
+        return send(rows.at[source], rows_all.at[source], z_send.at[d], z_recv.at[d], peer(sp=source))
+
+    def side_copies(d):
+        to = (tp + d) % 4
+        return (
+            send(mid, columns(tp), t_send.at[d, 0], t_recv.at[d, 0], peer(tp=to)),
+            send(down.at[to], down_all.at[tp], t_send.at[d, 1], t_recv.at[d, 1], peer(tp=to)),
+        )
+
+    def side_arrivals(d):
+        source = (tp - d + 4) % 4
+        return (
+            send(mid, columns(source), t_send.at[d, 0], t_recv.at[d, 0], peer(tp=source)),
+            send(down.at[source], down_all.at[source], t_send.at[d, 1], t_recv.at[d, 1], peer(tp=source)),
+        )
+
+    half = n_sp // 2
+    for d in sorted(range(1, n_sp), key=lambda d: abs(d - half)):
+        row_copy(d).start()
+    for d in (2, 1, 3):
+        for copy in side_copies(d):
+            copy.start()
+    own = (
+        pltpu.make_async_copy(rows.at[me], rows_all.at[me], own_sem.at[0]),
+        pltpu.make_async_copy(mid, columns(tp), own_sem.at[1]),
+    )
+    for copy in own:
+        copy.start()
+    for d in range(1, n_sp):
+        row_arrival(d).wait_recv()
+        row_copy(d).wait_send()
+    for d in range(1, 4):
+        for copy in side_arrivals(d):
+            copy.wait_recv()
+        for copy in side_copies(d):
+            copy.wait_send()
+    for copy in own:
+        copy.wait()
+
+
+def return_kernel(n_sp, produced, final, stage, t_send, t_recv, z_send, z_recv, own_sem):
+    me = lax.axis_index("sp")
+    tp = lax.axis_index("tp")
+    for d in range(1, n_sp):
+        greet(peer(sp=(me + d) % n_sp))
+    for d in range(1, 4):
+        greet(peer(tp=(tp + d) % 4))
+    pl.semaphore_wait(pltpu.get_barrier_semaphore(), n_sp - 1 + 3)
+
+    def target(d):
+        return (me + d) % n_sp
+
+    def landing(d, owner):
+        return final.at[me, owner] if d == 0 else stage.at[target(d), owner]
+
+    def side_copy(d, r):
+        to = (tp + r) % 4
+        return send(
+            produced.at[to, target(d)], landing(d, tp), t_send.at[d, r], t_recv.at[d, r], peer(tp=to)
+        )
+
+    def side_arrival(d, r):
+        source = (tp - r + 4) % 4
+        return send(
+            produced.at[source, target(d)],
+            landing(d, source),
+            t_send.at[d, r],
+            t_recv.at[d, r],
+            peer(tp=source),
+        )
+
+    def back_copy(d, r):
+        owner = (tp - r + 4) % 4
+        src = produced.at[tp, target(d)] if r == 0 else stage.at[target(d), owner]
+        return send(
+            src, final.at[me, owner], z_send.at[d, r], z_recv.at[d, r], peer(sp=target(d))
+        )
+
+    def back_arrival(d, r):
+        owner = (tp - r + 4) % 4
+        source = (me - d + n_sp) % n_sp
+        return send(
+            produced.at[tp, source],
+            final.at[source, owner],
+            z_send.at[d, r],
+            z_recv.at[d, r],
+            peer(sp=source),
+        )
+
+    half = n_sp // 2
+    order = sorted(range(1, n_sp), key=lambda d: abs(d - half))
+    for d in order:
+        back_copy(d, 0).start()
+    for d in order + [0]:
+        for r in (2, 1, 3):
+            side_copy(d, r).start()
+    own = pltpu.make_async_copy(produced.at[tp, me], final.at[me, tp], own_sem)
+    own.start()
+    for d in order:
+        for r in (1, 3, 2):
+            side_arrival(d, r).wait_recv()
+            back_copy(d, r).start()
+    for r in range(1, 4):
+        side_arrival(0, r).wait_recv()
+    for d in range(n_sp):
+        for r in range(1, 4):
+            side_copy(d, r).wait_send()
+    for d in order:
+        for r in range(4):
+            back_arrival(d, r).wait_recv()
+            back_copy(d, r).wait_send()
+    own.wait()
+
+
+def attention_kernel(q_ref, k_ref, v_ref, g_ref, o_ref, top, total, summed):
+    me = lax.axis_index("sp")
+    heads = g_ref.shape[1]
+    rows = q_ref.shape[0]
+    dim = q_ref.shape[1] // heads
+    for h in range(heads):
+        top[h] = jnp.full(top.shape[1:], -1e30, jnp.float32)
+        total[h] = jnp.zeros(total.shape[1:], jnp.float32)
+        summed[h] = jnp.zeros(summed.shape[1:], jnp.float32)
+
+    def fold(j, masked):
+        for h in range(heads):
+            columns = slice(h * dim, (h + 1) * dim)
+            scores = lax.dot_general(
+                q_ref[:, columns],
+                k_ref[j, :, columns],
+                (((1,), (1,)), ((), ())),
+                preferred_element_type=jnp.float32,
+            )
+            scores = scores - g_ref[j, h : h + 1, :]
+            if masked:
+                row = lax.broadcasted_iota(jnp.int32, scores.shape, 0)
+                column = lax.broadcasted_iota(jnp.int32, scores.shape, 1)
+                scores = jnp.where(column <= row, scores, -jnp.inf)
+            old = top[h]
+            new = jnp.maximum(old, jnp.max(scores, axis=1, keepdims=True))
+            factor = jnp.exp(old - new)
+            weight = jnp.exp(scores - new)
+            total[h] = total[h] * factor + jnp.sum(weight, axis=1, keepdims=True)
+            summed[h] = summed[h] * factor + jnp.dot(
+                weight.astype(jnp.bfloat16), v_ref[j, :, columns], preferred_element_type=jnp.float32
+            )
+            top[h] = new
+
+    def one(j, carry):
+        fold(j, False)
+        return carry
+
+    lax.fori_loop(0, me, one, 0)
+    fold(me, True)
+    for h in range(heads):
+        o_ref[:, h * dim : (h + 1) * dim] = (summed[h] / total[h]).astype(o_ref.dtype)
+
+
+def fast_shards(
+    queries,
+    key_vectors,
+    value_vectors,
+    log_gate_sums,
+    residual,
+    out_weight,
+    norm_gain,
+    routes,
+    route_weight,
+    expert_gate,
+    expert_up,
+    expert_down,
+    shared_gate,
+    shared_up,
+    shared_down,
+):
+    n_sp = lax.axis_size("sp")
+    tp = lax.axis_index("tp")
+    tok_dev = queries.shape[0]
+    heads = log_gate_sums.shape[1]
+    local_width = residual.shape[1]
+    model_width = norm_gain.shape[0]
+    exp_dev = expert_gate.shape[0]
+    experts_all = exp_dev * n_sp
+    top_count = routes.shape[1]
+    capacity = 5 * tok_dev * top_count // (4 * experts_all)
+    depth = n_sp // 2
+
+    def like(shape, array):
+        return jax.ShapeDtypeStruct(shape, array.dtype)
+
+    gates = log_gate_sums.T
+    k_all, v_all, g_all, gate_all, up_all = pl.pallas_call(
+        functools.partial(kv_kernel, n_sp),
+        name="kv_share",
+        out_shape=(
+            like((n_sp,) + key_vectors.shape, key_vectors),
+            like((n_sp,) + value_vectors.shape, value_vectors),
+            like((n_sp,) + gates.shape, gates),
+            like(expert_gate.shape, expert_gate),
+            like(expert_up.shape, expert_up),
+        ),
+        in_specs=vmem_space(3) + any_space(2),
+        out_specs=tuple(any_space(5)),
+        scratch_shapes=[
+            pltpu.SemaphoreType.DMA((depth, 3)),
+            pltpu.SemaphoreType.DMA((depth, 3)),
+            pltpu.SemaphoreType.DMA((depth, 3)),
+            pltpu.SemaphoreType.DMA((depth, 3)),
+            pltpu.SemaphoreType.DMA((3, 2)),
+            pltpu.SemaphoreType.DMA((3, 2)),
+            pltpu.SemaphoreType.DMA((3,)),
+        ],
+        compiler_params=pltpu.CompilerParams(collective_id=1, has_side_effects=True),
+    )(key_vectors, value_vectors, gates, expert_gate, expert_up)
+
+    scaled = (queries.astype(jnp.float32) * HDIM ** (-0.5)).astype(jnp.bfloat16)
+    attended = pl.pallas_call(
+        attention_kernel,
+        name="attention",
+        out_shape=like(queries.shape, queries),
+        in_specs=vmem_space(4),
+        out_specs=pl.BlockSpec(memory_space=pltpu.VMEM),
+        scratch_shapes=[
+            pltpu.VMEM((heads, tok_dev, 1), jnp.float32),
+            pltpu.VMEM((heads, tok_dev, 1), jnp.float32),
+            pltpu.VMEM((heads, tok_dev, HDIM), jnp.float32),
+        ],
+        compiler_params=pltpu.CompilerParams(vmem_limit_bytes=40 * 1024 * 1024),
+    )(scaled, k_all, v_all, g_all)
+
+    flat_routes = routes.reshape(-1)
+    onehot = flat_routes[:, None] == jnp.arange(experts_all, dtype=jnp.int32)[None, :]
+    pairs = tok_dev * top_count
+    earlier = (
+        jnp.arange(pairs, dtype=jnp.int32)[None, :] < jnp.arange(pairs, dtype=jnp.int32)[:, None]
+    ).astype(jnp.bfloat16)
+    before = jnp.dot(earlier, onehot.astype(jnp.bfloat16), preferred_element_type=jnp.float32)
+    rank = jnp.sum(jnp.where(onehot, before, 0.0), axis=1).astype(jnp.int32)
+    rank = rank.reshape(tok_dev, top_count)
+    targets = routes * capacity + rank
+    here = jnp.where(routes % exp_dev == tp, routes // exp_dev * capacity + rank, -1)
+    slots = jnp.arange(n_sp * capacity, dtype=jnp.int32)[:, None]
+    chosen = slots == here[:, 0][None, :]
+    for k in range(1, top_count):
+        chosen = chosen | (slots == here[:, k][None, :])
+    chosen = chosen.astype(jnp.bfloat16)
+
+    attended_all = gather_features(attended, 2)
+    projected = jnp.dot(attended_all, out_weight, preferred_element_type=jnp.float32)
+    mid = (residual.astype(jnp.float32) + projected).astype(jnp.bfloat16)
+    mid_all = gather_features(mid, 3).astype(jnp.float32)
+    inverse = lax.rsqrt(jnp.mean(mid_all * mid_all, axis=1, keepdims=True) + EPSILON)
+    normed = (mid_all * inverse * norm_gain.astype(jnp.float32)[None, :]).astype(jnp.bfloat16)
+    rows = jnp.dot(chosen, normed, preferred_element_type=jnp.float32).astype(jnp.bfloat16)
+    rows = rows.reshape(n_sp, capacity, model_width)
+    shared_mid = silu_gate(
+        jnp.dot(normed, shared_gate, preferred_element_type=jnp.float32),
+        jnp.dot(normed, shared_up, preferred_element_type=jnp.float32),
+    ).astype(jnp.bfloat16)
+
+    rows_all, shared_all, down_all = pl.pallas_call(
+        functools.partial(dispatch_kernel, n_sp),
+        name="dispatch",
+        out_shape=(
+            like(rows.shape, rows),
+            like((tok_dev, 4 * shared_mid.shape[1]), shared_mid),
+            like(expert_down.shape, expert_down),
+        ),
+        in_specs=vmem_space(2) + any_space(1),
+        out_specs=tuple(any_space(3)),
+        scratch_shapes=[
+            pltpu.SemaphoreType.DMA((n_sp,)),
+            pltpu.SemaphoreType.DMA((n_sp,)),
+            pltpu.SemaphoreType.DMA((4, 2)),
+            pltpu.SemaphoreType.DMA((4, 2)),
+            pltpu.SemaphoreType.DMA((2,)),
+        ],
+        compiler_params=pltpu.CompilerParams(collective_id=4, has_side_effects=True),
+    )(rows, shared_mid, expert_down)
+
+    def with_own(whole, shard):
+        block = lax.dynamic_slice_in_dim(shard, tp, 1, 0)
+        return lax.dynamic_update_slice_in_dim(whole, block, tp, 0)
+
+    gate_all = with_own(gate_all, expert_gate)
+    up_all = with_own(up_all, expert_up)
+    down_all = with_own(down_all, expert_down)
+    flat_rows = rows_all.reshape(n_sp * capacity, model_width)
+    hidden = jnp.concatenate(
+        [
+            silu_gate(
+                jnp.dot(flat_rows, gate_all[t], preferred_element_type=jnp.float32),
+                jnp.dot(flat_rows, up_all[t], preferred_element_type=jnp.float32),
+            ).astype(jnp.bfloat16)
+            for t in range(4)
+        ],
+        axis=1,
+    )
+    produced = jnp.stack(
+        [
+            jnp.dot(hidden, down_all[t], preferred_element_type=jnp.float32).astype(jnp.bfloat16)
+            for t in range(4)
+        ]
+    ).reshape(4, n_sp, capacity, local_width)
+
+    final = pl.pallas_call(
+        functools.partial(return_kernel, n_sp),
+        name="give_back",
+        out_shape=like((n_sp, 4, capacity, local_width), produced),
+        in_specs=vmem_space(1),
+        out_specs=pl.BlockSpec(memory_space=pl.ANY),
+        scratch_shapes=[
+            pltpu.VMEM((n_sp, 4, capacity, local_width), jnp.bfloat16),
+            pltpu.SemaphoreType.DMA((n_sp, 4)),
+            pltpu.SemaphoreType.DMA((n_sp, 4)),
+            pltpu.SemaphoreType.DMA((n_sp, 4)),
+            pltpu.SemaphoreType.DMA((n_sp, 4)),
+            pltpu.SemaphoreType.DMA,
+        ],
+        compiler_params=pltpu.CompilerParams(collective_id=5, has_side_effects=True),
+    )(produced)
+
+    shared_out = jnp.dot(shared_all, shared_down, preferred_element_type=jnp.float32)
+    returned = final.reshape(experts_all * capacity, local_width)
+    places = jnp.arange(experts_all * capacity, dtype=jnp.int32)[None, :]
+    result = mid.astype(jnp.float32) + shared_out
+    for k in range(top_count):
+        pick = (places == targets[:, k][:, None]).astype(jnp.bfloat16)
+        picked = jnp.dot(pick, returned, preferred_element_type=jnp.float32)
+        result = result + picked * route_weight[:, k][:, None]
+    return result.astype(jnp.bfloat16)
+
+
 def solution(mesh):
     placed = (
         P("sp", "tp"),
@@ -187,6 +803,7 @@
         P(None, "tp"),
         P(None, "tp"),
     )
+    fits = mesh.shape["tp"] == 4 and mesh.shape["sp"] % 2 == 0 and mesh.shape["sp"] <= 16
     return jax.shard_map(
-        shards, mesh=mesh, in_specs=placed, out_specs=P("sp", "tp"), check_vma=False
-    )
+        fast_shards if fits else shards, mesh=mesh, in_specs=placed, out_specs=P("sp", "tp"), check_vma=False
+    )

time: 385 us -> 230 us (0.60); the launches traced: 380 us -> 230 us
  Pallas kernels: 0 us -> 192 us
  waiting for transfers between devices: 192 us -> 0 us
  blocking collectives: 67.3 us -> 0 us
  local copies, waits for them, and re-layouts: 38.5 us -> 11.7 us
  other arithmetic: 21.9 us -> 4.6 us
  between operations: 13.8 us -> 0.41 us
  matrix products: 34.4 us -> 21.2 us
  starting transfers between devices: 5.98 us -> 0 us
  loops' own time: 5.81 us -> 0 us
    all_gather x6 -> x0, waiting for transfers between devices: 192 us -> none  [the longest x1 61.1 us: shards(): lax.all_gather(lax.all_to_all(outgoing, 'sp', split_axis=0, concat_axis=0...]
    pallas_call x0 -> x6, Pallas kernels: none -> 192 us  [the longest x1 55.3 us: fast_shards(): pl.pallas_call(functools.partial(dispatch_kernel, n_sp), name='dispatch',...]
    all_to_all x1 -> x0, blocking collectives: 36.8 us -> none  [shards(): lax.all_to_all(outgoing, 'sp', split_axis=0, concat_axis=0, tiled=True)]
    all_gather x2 -> x0, blocking collectives: 23.6 us -> none  [the longest x1 15 us: shards(): all_gates = lax.all_gather(log_gate_sums, 'sp', axis=0, tiled=True)]
    dot_general x15 -> x20, matrix products: 34.4 us -> 21.2 us  [the longest x2 3.99 us: fast_shards(): picked = jnp.dot(pick, returned, preferred_element_type=jnp.float32)]
    gather x2 -> x0, local copies, waits for them, and re-layouts: 9.8 us -> none  [the longest x1 5.07 us: shards(): returned_flat[targets].astype(jnp.float32)]
    another operation x3 -> x1, other arithmetic: 9.14 us -> 1.23 us  [fast_shards(): jnp.stack([jnp.dot(hidden, down_all[t], preferred_element_type=jnp.float3...]
    reduce_sum x6 -> x1, other arithmetic: 10 us -> 2.22 us  [fast_shards(): jnp.mean(mid_all * mid_all, axis=1, keepdims=True) + EPSILON]
  transfers between devices with their start and end apart: 7 -> 0, of which waited for: 6 -> 0; matrix products, arithmetic and copies ran while one was open for 8% -> 0% of each run, Pallas kernels for 0% -> 0%
where the time goes in v1:
time: 230 us
  Pallas kernels  192 us (83%)
  matrix products  21.2 us (9%)
  local copies, waits for them, and re-layouts  11.7 us (5%)
  other arithmetic  4.6 us (2%)
    pallas_call x1, Pallas kernels, fast_shards(): pl.pallas_call(functools.partial(dispatch_kernel, n_sp), name='dispatch',...  55.3 us
    pallas_call x1, Pallas kernels, fast_shards(): pl.pallas_call(functools.partial(kv_kernel, n_sp), name='kv_share', out_s...  49.6 us
    pallas_call x1, Pallas kernels, fast_shards(): pl.pallas_call(functools.partial(return_kernel, n_sp), name='give_back',...  34.4 us
    pallas_call x2, Pallas kernels, gather_features(): pl.pallas_call(gather_kernel, name=f'gather_{number}', out_shape=jax.Shap...  29.5 us
    pallas_call x1, Pallas kernels, fast_shards(): pl.pallas_call(attention_kernel, name='attention', out_shape=like(queries...  22.7 us
    unnamed x41, local copies, waits for them, and re-layouts  6.2 us

profile of v1, /device:TPU:9, one launch (start us, length us, event | category | flops | bytes accessed | tf_op | source)
XLA Modules:
  0.0 229.5 jit_solution(4734486009912388877)
XLA Ops:
  0.0 0.8 broadcast_multiply_fusion
  1.0 0.8 copy.27
  2.0 0.5 fusion.20
  3.2 0.5 slice_reduce_fusion
  3.8 49.6 %kv_share.1 = (bf16[8,512,256]{2,1,0:T(8,128)(2,1)}, bf16[8,512,256]{2,1,0:T(8,128)(2,1)}, f32[8,4,512]{2,1,0:T(4,128)}, bf16[4,2048,128]{2,1,0:T(8,128)(2,1)}, bf16[4,2048,128]{2,1,0:T(8,128)(2,1)}) custom-call(bf16[512,256]{1,0:T(8,128)(2,1)} %k_ref.1, bf16[512,256]{1,0:T(8,128)(2,1)} %v_ref.1, f32[4,512]{1,0:T(4,128)} %bitcast.69, ...), custom_call_target="tpu_custom_call" | custom-call | tf_op jit(solution)/shard_map/kv_share/pallas_call | solution.py:646
  53.5 1.6 copy-done.1
  55.1 1.6 copy-done.2
  56.7 0.8 copy-done.4
  57.5 22.7 %attention.1.block = bf16[512,256]{1,0:T(8,128)(2,1)S(1)} custom-call(bf16[512,256]{1,0:T(8,128)(2,1)S(1)} %multiply_convert_fusion.q_ref, bf16[8,512,256]{2,1,0:T(8,128)(2,1)S(1)} %copy-done.1, bf16[8,512,256]{2,1,0:T(8,128)(2,1)S(1)} %copy-done.2, f32[8,4,512]{2,1,0:T(4,128)S(1)} %copy-done.4), custom_call_target="tpu_custom_call" | custom-call | tf_op jit(solution)/shard_map/attention/pallas_call | solution.py:671
  80.2 0.7 copy-done.3
  80.9 10.8 %gather_2.1 = bf16[512,1024]{1,0:T(8,128)(2,1)} custom-call(bf16[512,256]{1,0:T(8,128)(2,1)} %copy-done.3), custom_call_target="tpu_custom_call" | custom-call | tf_op jit(solution)/shard_map/gather_2/pallas_call | solution.py:419
  91.7 2.7 %fusion.12.block = bf16[512,512]{1,0:T(8,128)(2,1)} fusion(bf16[512,1024]{1,0:T(8,128)(2,1)} %gather_2.1, bf16[1024,512]{1,0:T(8,128)(2,1)S(1)} %copy-done, bf16[512,512]{1,0:T(8,128)(2,1)S(1)} %copy-done.17), kind=kOutput, calls=%fused_computation.21 | convolution fusion | flops 537657344 | bytes 3145728 | tf_op jit(solution)/shard_map/dot_general | solution.py:703
  94.4 18.7 %gather_3.1 = bf16[512,2048]{1,0:T(8,128)(2,1)} custom-call(bf16[512,512]{1,0:T(8,128)(2,1)} %fusion.12.block), custom_call_target="tpu_custom_call" | custom-call | tf_op jit(solution)/shard_map/gather_3/pallas_call | solution.py:419
  113.2 2.2 fusion
  115.5 2.3 convolution_convert_fusion
  117.7 0.8 fusion.37
  118.8 1.4 fusion.14.mid
  120.2 55.3 %dispatch.1 = (bf16[8,40,2048]{2,1,0:T(8,128)(2,1)}, bf16[512,512]{1,0:T(8,128)(2,1)}, bf16[4,512,512]{2,1,0:T(8,128)(2,1)}) custom-call(bf16[8,40,2048]{2,1,0:T(8,128)(2,1)} %bitcast.62, bf16[512,128]{1,0:T(8,128)(2,1)} %fusion.14.mid, bf16[4,512,512]{2,1,0:T(8,128)(2,1)} %down.1), custom_call_target="tpu_custom_call" | custom-call | tf_op jit(solution)/shard_map/dispatch/pallas_call | solution.py:715
  175.6 1.5 convolution_add_fusion
  177.1 2.0 dynamic-slice_dynamic-update-slice_fusion
  179.1 2.3 dynamic-slice_dynamic-update-slice_fusion.1
  181.4 1.7 fusion.23
  183.1 1.7 fusion.19
  184.8 0.5 fusion.24
  185.3 0.5 fusion.18
  186.3 0.5 fusion.17
  186.9 0.5 fusion.26
  187.4 0.7 fusion.16
  189.8 1.2 pad_maximum_fusion.produced
  191.1 34.4 %give_back.1 = bf16[8,4,40,512]{3,2,1,0:T(8,128)(2,1)} custom-call(bf16[4,8,40,512]{3,2,1,0:T(8,128)(2,1)} %pad_maximum_fusion.produced), custom_call_target="tpu_custom_call" | custom-call | tf_op jit(solution)/shard_map/give_back/pallas_call | solution.py:760
  225.5 2.3 %fusion.9 = f32[512,512]{1,0:T(8,128)S(1)} fusion(f32[512,512]{1,0:T(8,128)S(1)} %convolution_add_fusion, bf16[1280,512]{1,0:T(8,128)(2,1)} %bitcast.63, s32[512]{0:T(512)S(1)} %get-tuple-element.22, f32[512]{0:T(512)S(1)} %bitcast.71), kind=kOutput, calls=%fused_computation.15 | convolution fusion | flops 672268288 | bytes 3411968 | tf_op jit(solution)/shard_map/dot_general | solution.py:783
  227.8 1.7 fusion.13
  (52 shorter events, 3.6 us)
Async XLA Ops:
  0.0 91.7 %copy-start = (bf16[1024,512]{1,0:T(8,128)(2,1)S(1)}, bf16[1024,512]{1,0:T(8,128)(2,1)}, u32[]{:S(2)}) copy-start(bf16[1024,512]{1,0:T(8,128)(2,1)} %param.20) | copy-start | bytes 3145732
  0.0 2.7 %copy-start.10 = (s32[512,2]{0,1:T(2,128)S(1)}, s32[512,2]{0,1:T(2,128)}, u32[]{:S(2)}) copy-start(s32[512,2]{0,1:T(2,128)} %param.22) | copy-start | bytes 12292
  2.0 1.8 copy-start.9
  53.5 1.6 copy-start.1
  55.1 1.6 copy-start.2
  56.7 0.8 copy-start.4
  57.5 34.2 %copy-start.17 = (bf16[512,512]{1,0:T(8,128)(2,1)S(1)}, bf16[512,512]{1,0:T(8,128)(2,1)}, u32[]{:S(2)}) copy-start(bf16[512,512]{1,0:T(8,128)(2,1)} %param.19) | copy-start | bytes 1572868
  80.2 0.7 copy-start.3
  94.4 18.7 %copy-start.11 = (bf16[2048]{0:T(1024)(128)(2,1)S(1)}, bf16[2048]{0:T(1024)(128)(2,1)}, u32[]{:S(2)}) copy-start(bf16[2048]{0:T(1024)(128)(2,1)} %param.21) | copy-start | bytes 12292
  113.2 2.3 copy-start.5
  115.4 2.3 copy-start.18
  117.7 1.0 copy-start.19
  120.2 55.3 %copy-start.6 = (bf16[512,512]{1,0:T(8,128)(2,1)S(1)}, bf16[512,512]{1,0:T(8,128)(2,1)}, u32[]{:S(2)}) copy-start(bf16[512,512]{1,0:T(8,128)(2,1)} %fusion.12.block) | copy-start | bytes 1572868
  120.2 55.4 %copy-start.8 = (bf16[512,512]{1,0:T(8,128)(2,1)S(1)}, bf16[512,512]{1,0:T(8,128)(2,1)}, u32[]{:S(2)}) copy-start(bf16[512,512]{1,0:T(8,128)(2,1)} %param.29) | copy-start | bytes 1572868
  177.1 4.3 %copy-start.16 = (bf16[8,40,2048]{2,1,0:T(8,128)(2,1)S(1)}, bf16[8,40,2048]{2,1,0:T(8,128)(2,1)}, u32[]{:S(2)}) copy-start(bf16[8,40,2048]{2,1,0:T(8,128)(2,1)} %get-tuple-element.17) | copy-start | bytes 3932164
  181.3 3.4 %copy-start.13 = (bf16[4,2048,128]{2,1,0:T(8,128)(2,1)S(1)}, bf16[4,2048,128]{2,1,0:T(8,128)(2,1)}, u32[]{:S(2)}) copy-start(bf16[4,2048,128]{2,1,0:T(8,128)(2,1)} %get-tuple-element.32) | copy-start | bytes 6291460
  183.1 2.3 copy-start.14
  186.9 1.6 copy-start.15
  189.8 35.7 %copy-start.12 = (f32[512,2]{0,1:T(2,128)S(1)}, f32[512,2]{0,1:T(2,128)}, u32[]{:S(2)}) copy-start(f32[512,2]{0,1:T(2,128)} %param.23) | copy-start | bytes 12292
  225.5 2.3 %copy-start.7 = (bf16[8,4,40,512]{3,2,1,0:T(8,128)(2,1)S(1)}, bf16[8,4,40,512]{3,2,1,0:T(8,128)(2,1)}, u32[]{:S(2)}) copy-start(bf16[8,4,40,512]{3,2,1,0:T(8,128)(2,1)} %give_back.1) | copy-start | bytes 3932164

commit v2 on v1

--- a/solution.py
+++ b/solution.py
@@ -454,26 +454,43 @@
         source = (me - d + n_sp) % n_sp
         return send(rows.at[source], rows_all.at[source], z_send.at[d], z_recv.at[d], peer(sp=source))
 
+    half = down.shape[1] // 2
+
     def side_copies(d):
         to = (tp + d) % 4
-        return (
-            send(mid, columns(tp), t_send.at[d, 0], t_recv.at[d, 0], peer(tp=to)),
-            send(down.at[to], down_all.at[tp], t_send.at[d, 1], t_recv.at[d, 1], peer(tp=to)),
-        )
+        return [send(mid, columns(tp), t_send.at[d, 0], t_recv.at[d, 0], peer(tp=to))] + [
+            send(
+                down.at[to, pl.ds(i * half, half)],
+                down_all.at[tp, pl.ds(i * half, half)],
+                t_send.at[d, 1 + i],
+                t_recv.at[d, 1 + i],
+                peer(tp=to),
+            )
+            for i in range(2)
+        ]
 
     def side_arrivals(d):
         source = (tp - d + 4) % 4
-        return (
-            send(mid, columns(source), t_send.at[d, 0], t_recv.at[d, 0], peer(tp=source)),
-            send(down.at[source], down_all.at[source], t_send.at[d, 1], t_recv.at[d, 1], peer(tp=source)),
-        )
-
-    half = n_sp // 2
-    for d in sorted(range(1, n_sp), key=lambda d: abs(d - half)):
-        row_copy(d).start()
-    for d in (2, 1, 3):
-        for copy in side_copies(d):
-            copy.start()
+        return [send(mid, columns(source), t_send.at[d, 0], t_recv.at[d, 0], peer(tp=source))] + [
+            send(
+                down.at[source, pl.ds(i * half, half)],
+                down_all.at[source, pl.ds(i * half, half)],
+                t_send.at[d, 1 + i],
+                t_recv.at[d, 1 + i],
+                peer(tp=source),
+            )
+            for i in range(2)
+        ]
+
+    middle = n_sp // 2
+    groups = [side_copies(d) for d in (2, 1, 3)]
+    sides = [group[i] for i in range(3) for group in groups]
+    straight = [row_copy(d) for d in sorted(range(1, n_sp), key=lambda d: abs(d - middle))]
+    for i in range(max(len(sides), len(straight))):
+        if i < len(straight):
+            straight[i].start()
+        if i < len(sides):
+            sides[i].start()
     own = (
         pltpu.make_async_copy(rows.at[me], rows_all.at[me], own_sem.at[0]),
         pltpu.make_async_copy(mid, columns(tp), own_sem.at[1]),
@@ -608,6 +625,36 @@
     fold(me, True)
     for h in range(heads):
         o_ref[:, h * dim : (h + 1) * dim] = (summed[h] / total[h]).astype(o_ref.dtype)
+
+
+def expert_kernel(
+    rows, gate_own, up_own, down_own, gate_all, up_all, down_all, produced, gate, up, down, sems
+):
+    tp = lax.axis_index("tp")
+    owns, wholes, targets = (gate_own, up_own, down_own), (gate_all, up_all, down_all), (gate, up, down)
+    copies = []
+    for i in range(3):
+        width = owns[i].shape[2]
+        for d in range(4):
+            source = (tp + d) % 4
+            src = owns[i].at[tp] if d == 0 else wholes[i].at[source]
+            columns = pl.ds(pl.multiple_of(source * width, width), width)
+            copies.append(pltpu.make_async_copy(src, targets[i].at[:, columns], sems.at[i, d]))
+            copies[-1].start()
+    for copy in copies[:4]:
+        copy.wait()
+    gate_part = jnp.dot(rows[...], gate[...], preferred_element_type=jnp.float32)
+    for copy in copies[4:8]:
+        copy.wait()
+    up_part = jnp.dot(rows[...], up[...], preferred_element_type=jnp.float32)
+    hidden = silu_gate(gate_part, up_part).astype(jnp.bfloat16)
+    for copy in copies[8:]:
+        copy.wait()
+    width = produced.shape[2]
+    for t in range(4):
+        produced[t] = jnp.dot(
+            hidden, down[:, t * width : (t + 1) * width], preferred_element_type=jnp.float32
+        ).astype(produced.dtype)
 
 
 def fast_shards(
@@ -725,36 +772,34 @@
         scratch_shapes=[
             pltpu.SemaphoreType.DMA((n_sp,)),
             pltpu.SemaphoreType.DMA((n_sp,)),
-            pltpu.SemaphoreType.DMA((4, 2)),
-            pltpu.SemaphoreType.DMA((4, 2)),
+            pltpu.SemaphoreType.DMA((4, 3)),
+            pltpu.SemaphoreType.DMA((4, 3)),
             pltpu.SemaphoreType.DMA((2,)),
         ],
         compiler_params=pltpu.CompilerParams(collective_id=4, has_side_effects=True),
     )(rows, shared_mid, expert_down)
 
-    def with_own(whole, shard):
-        block = lax.dynamic_slice_in_dim(shard, tp, 1, 0)
-        return lax.dynamic_update_slice_in_dim(whole, block, tp, 0)
-
-    gate_all = with_own(gate_all, expert_gate)
-    up_all = with_own(up_all, expert_up)
-    down_all = with_own(down_all, expert_down)
-    flat_rows = rows_all.reshape(n_sp * capacity, model_width)
-    hidden = jnp.concatenate(
-        [
-            silu_gate(
-                jnp.dot(flat_rows, gate_all[t], preferred_element_type=jnp.float32),
-                jnp.dot(flat_rows, up_all[t], preferred_element_type=jnp.float32),
-            ).astype(jnp.bfloat16)
-            for t in range(4)
+    produced = pl.pallas_call(
+        expert_kernel,
+        name="experts",
+        out_shape=like((4, n_sp * capacity, local_width), rows),
+        in_specs=vmem_space(1) + any_space(6),
+        out_specs=pl.BlockSpec(memory_space=pltpu.VMEM),
+        scratch_shapes=[
+            pltpu.VMEM((model_width, 4 * expert_gate.shape[2]), jnp.bfloat16),
+            pltpu.VMEM((model_width, 4 * expert_up.shape[2]), jnp.bfloat16),
+            pltpu.VMEM((expert_down.shape[1], 4 * expert_down.shape[2]), jnp.bfloat16),
+            pltpu.SemaphoreType.DMA((3, 4)),
         ],
-        axis=1,
-    )
-    produced = jnp.stack(
-        [
-            jnp.dot(hidden, down_all[t], preferred_element_type=jnp.float32).astype(jnp.bfloat16)
-            for t in range(4)
-        ]
+        compiler_params=pltpu.CompilerParams(vmem_limit_bytes=40 * 1024 * 1024),
+    )(
+        rows_all.reshape(n_sp * capacity, model_width),
+        expert_gate,
+        expert_up,
+        expert_down,
+        gate_all,
+        up_all,
+        down_all,
     ).reshape(4, n_sp, capacity, local_width)
 
     final = pl.pallas_call(

time: 230 us -> 229 us (level)
  matrix products: 21.2 us -> 11.8 us
  local copies, waits for them, and re-layouts: 11.7 us -> 17.1 us
  Pallas kernels: 192 us -> 196 us
    unnamed x41 -> x47, local copies, waits for them, and re-layouts: 6.2 us -> 14.5 us
    dot_general x12 -> x0, matrix products: 8.02 us -> none  [the longest x4 3.48 us: fast_shards(): jnp.dot(flat_rows, up_all[t], preferred_element_type=jnp.float32)]
    dynamic_update_slice x2 -> x0, local copies, waits for them, and re-layouts: 4.28 us -> none  [with_own(): return lax.dynamic_update_slice_in_dim(whole, block, tp, 0)]
    pallas_call x0 -> x1, Pallas kernels: none -> 3.7 us  [fast_shards(): pl.pallas_call(expert_kernel, name='experts', out_shape=like((4, n_sp * c...]
where the time goes in v2:
time: 229 us
  Pallas kernels  196 us (86%)
  local copies, waits for them, and re-layouts  17.1 us (7%)
  matrix products  11.8 us (5%)
  other arithmetic  3.61 us (2%)
    pallas_call x1, Pallas kernels, fast_shards(): pl.pallas_call(functools.partial(dispatch_kernel, n_sp), name='dispatch',...  55.5 us
    pallas_call x1, Pallas kernels, fast_shards(): pl.pallas_call(functools.partial(kv_kernel, n_sp), name='kv_share', out_s...  49.7 us
    pallas_call x1, Pallas kernels, fast_shards(): pl.pallas_call(functools.partial(return_kernel, n_sp), name='give_back',...  34.6 us
    pallas_call x2, Pallas kernels, gather_features(): pl.pallas_call(gather_kernel, name=f'gather_{number}', out_shape=jax.Shap...  29.6 us
    pallas_call x1, Pallas kernels, fast_shards(): pl.pallas_call(attention_kernel, name='attention', out_shape=like(queries...  22.6 us
    unnamed x47, local copies, waits for them, and re-layouts  14.5 us

profile of v2, /device:TPU:9, one launch (start us, length us, event | category | flops | bytes accessed | tf_op | source)
XLA Modules:
  0.0 228.5 jit_solution(7665851671164057609)
XLA Ops:
  0.0 49.7 %kv_share.1 = (bf16[8,512,256]{2,1,0:T(8,128)(2,1)}, bf16[8,512,256]{2,1,0:T(8,128)(2,1)}, f32[8,4,512]{2,1,0:T(4,128)}, bf16[4,2048,128]{2,1,0:T(8,128)(2,1)}, bf16[4,2048,128]{2,1,0:T(8,128)(2,1)}) custom-call(bf16[512,256]{1,0:T(8,128)(2,1)} %k_ref.1, bf16[512,256]{1,0:T(8,128)(2,1)} %v_ref.1, f32[4,512]{1,0:T(4,128)} %bitcast.20, ...), custom_call_target="tpu_custom_call" | custom-call | tf_op jit(solution)/shard_map/kv_share/pallas_call | solution.py:693
  49.8 1.6 copy-done.5
  51.4 1.6 copy-done.6
  53.0 0.8 copy-done.11
  53.8 22.6 %attention.1.block = bf16[512,256]{1,0:T(8,128)(2,1)S(1)} custom-call(bf16[512,256]{1,0:T(8,128)(2,1)S(1)} %multiply_convert_fusion.q_ref, bf16[8,512,256]{2,1,0:T(8,128)(2,1)S(1)} %copy-done.5, bf16[8,512,256]{2,1,0:T(8,128)(2,1)S(1)} %copy-done.6, f32[8,4,512]{2,1,0:T(4,128)S(1)} %copy-done.11), custom_call_target="tpu_custom_call" | custom-call | tf_op jit(solution)/shard_map/attention/pallas_call | solution.py:718
  76.5 0.7 copy-done.10
  77.2 10.8 %gather_2.1 = bf16[512,1024]{1,0:T(8,128)(2,1)} custom-call(bf16[512,256]{1,0:T(8,128)(2,1)} %copy-done.10), custom_call_target="tpu_custom_call" | custom-call | tf_op jit(solution)/shard_map/gather_2/pallas_call | solution.py:419
  88.0 2.7 %fusion.12.block = bf16[512,512]{1,0:T(8,128)(2,1)} fusion(bf16[512,1024]{1,0:T(8,128)(2,1)} %gather_2.1, bf16[1024,512]{1,0:T(8,128)(2,1)S(1)} %copy-done, bf16[512,512]{1,0:T(8,128)(2,1)S(1)} %copy-done.21), kind=kOutput, calls=%fused_computation.20 | convolution fusion | flops 537657344 | bytes 3145728 | tf_op jit(solution)/shard_map/dot_general | solution.py:750
  90.8 18.7 %gather_3.1 = bf16[512,2048]{1,0:T(8,128)(2,1)} custom-call(bf16[512,512]{1,0:T(8,128)(2,1)} %fusion.12.block), custom_call_target="tpu_custom_call" | custom-call | tf_op jit(solution)/shard_map/gather_3/pallas_call | solution.py:419
  109.5 2.2 fusion
  111.8 1.9 fusion.29
  113.7 1.4 fusion.14.mid
  115.4 0.5 fusion.16
  116.0 0.9 convert_element_type.51
  116.9 0.9 copy.35
  117.8 0.2 copy.30
  118.0 1.3 fusion.32
  119.3 0.5 slice_reduce_fusion
  119.8 2.3 convolution_convert_fusion
  122.0 55.5 %dispatch.1 = (bf16[8,40,2048]{2,1,0:T(8,128)(2,1)}, bf16[512,512]{1,0:T(8,128)(2,1)}, bf16[4,512,512]{2,1,0:T(8,128)(2,1)}) custom-call(bf16[8,40,2048]{2,1,0:T(8,128)(2,1)} %bitcast.17, bf16[512,128]{1,0:T(8,128)(2,1)} %fusion.14.mid, bf16[4,512,512]{2,1,0:T(8,128)(2,1)} %down_own.1), custom_call_target="tpu_custom_call" | custom-call | tf_op jit(solution)/shard_map/dispatch/pallas_call | solution.py:762
  177.6 1.6 copy-done.2
  179.1 1.6 copy-done.3
  180.7 1.6 copy-done.7
  182.3 1.6 copy-done.8
  183.9 1.3 copy-done.9
  185.2 3.7 %experts.1 = bf16[4,320,512]{2,1,0:T(8,128)(2,1)S(1)} custom-call(bf16[320,2048]{1,0:T(8,128)(2,1)S(1)} %bitcast.16, bf16[4,2048,128]{2,1,0:T(8,128)(2,1)S(1)} %copy-done.2, bf16[4,2048,128]{2,1,0:T(8,128)(2,1)S(1)} %copy-done.3, bf16[4,512,512]{2,1,0:T(8,128)(2,1)S(1)} %copy-done.1, bf16[4,2048,128]{2,1,0:T(8,128)(2,1)S(1)} %copy-done.7, ...), custom_call_target="tpu_custom_call" | custom-call | tf_op jit(solution)/shard_map/experts/pallas_call | solution.py:782
  188.9 1.1 copy-done.4
  190.0 34.6 %give_back.1 = bf16[8,4,40,512]{3,2,1,0:T(8,128)(2,1)} custom-call(bf16[4,8,40,512]{3,2,1,0:T(8,128)(2,1)} %bitcast.15), custom_call_target="tpu_custom_call" | custom-call | tf_op jit(solution)/shard_map/give_back/pallas_call | solution.py:805
  224.7 0.4 convolution_add_fusion
  225.1 0.8 copy-done.14
  226.0 0.9 fusion.9
  226.9 1.7 fusion.13
  (44 shorter events, 0.5 us)
Async XLA Ops:
  0.0 88.0 %copy-start = (bf16[1024,512]{1,0:T(8,128)(2,1)S(1)}, bf16[1024,512]{1,0:T(8,128)(2,1)}, u32[]{:S(2)}) copy-start(bf16[1024,512]{1,0:T(8,128)(2,1)} %param.20) | copy-start | bytes 3145732
  0.0 49.7 %copy-start.17 = (bf16[512,256]{1,0:T(8,128)(2,1)S(1)}, bf16[512,256]{1,0:T(8,128)(2,1)}, u32[]{:S(2)}) copy-start(bf16[512,256]{1,0:T(8,128)(2,1)} %param.15) | copy-start | bytes 786436
  49.8 1.6 copy-start.5
  51.4 1.6 copy-start.6
  53.0 0.8 copy-start.11
  53.8 34.2 %copy-start.21 = (bf16[512,512]{1,0:T(8,128)(2,1)S(1)}, bf16[512,512]{1,0:T(8,128)(2,1)}, u32[]{:S(2)}) copy-start(bf16[512,512]{1,0:T(8,128)(2,1)} %param.19) | copy-start | bytes 1572868
  76.5 0.7 copy-start.10
  90.8 21.0 %copy-start.19 = (bf16[2048]{0:T(1024)(128)(2,1)S(1)}, bf16[2048]{0:T(1024)(128)(2,1)}, u32[]{:S(2)}) copy-start(bf16[2048]{0:T(1024)(128)(2,1)} %param.21) | copy-start | bytes 12292
  109.5 2.3 copy-start.12
  111.8 1.9 copy-start.22
  113.7 1.4 copy-start.18
  122.0 55.5 %copy-start.1 = (bf16[4,512,512]{2,1,0:T(8,128)(2,1)S(1)}, bf16[4,512,512]{2,1,0:T(8,128)(2,1)}, u32[]{:S(2)}) copy-start(bf16[4,512,512]{2,1,0:T(8,128)(2,1)} %down_own.1) | copy-start | bytes 6291460
  177.5 1.6 copy-start.2
  179.1 1.6 copy-start.3
  180.7 1.6 copy-start.7
  182.3 1.6 copy-start.8
  183.9 1.3 copy-start.9
  188.9 1.1 copy-start.4
  190.0 34.6 %copy-start.13 = (bf16[512,512]{1,0:T(8,128)(2,1)S(1)}, bf16[512,512]{1,0:T(8,128)(2,1)}, u32[]{:S(2)}) copy-start(bf16[512,512]{1,0:T(8,128)(2,1)} %fusion.12.block) | copy-start | bytes 1572868
  190.0 34.7 %copy-start.15 = (bf16[512,512]{1,0:T(8,128)(2,1)S(1)}, bf16[512,512]{1,0:T(8,128)(2,1)}, u32[]{:S(2)}) copy-start(bf16[512,512]{1,0:T(8,128)(2,1)} %param.29) | copy-start | bytes 1572868
  190.0 34.7 %copy-start.16 = (bf16[512,512]{1,0:T(8,128)(2,1)S(1)}, bf16[512,512]{1,0:T(8,128)(2,1)}, u32[]{:S(2)}) copy-start(bf16[512,512]{1,0:T(8,128)(2,1)} %get-tuple-element.16) | copy-start | bytes 1572868
  190.0 35.1 %copy-start.20 = (f32[512,2]{0,1:T(2,128)S(1)}, f32[512,2]{0,1:T(2,128)}, u32[]{:S(2)}) copy-start(f32[512,2]{0,1:T(2,128)} %param.23) | copy-start | bytes 12292
  224.6 1.3 copy-start.14
